TPU v7x, 256 devices: a 4x2x16 block of a 4x16x16 slice. The times are simulated.
256 devices in a mesh: grp: 2 (over y), st: 32 (over z, core), tp: 4 (over x).
Axes of the slice: x: 4, y: 2, z: 16, core: 2. Of those that a mesh axis runs over, the one named last changes fastest.
The devices are a block of a 4x16x16 slice.
Arguments:
- pass_ids: int32 [512, 4], P(('grp', 'st')), parts along dimension 0, may hold values from 0 to 511, as said below
- store: bfloat16 [512, 64, 2048], P('st', None, 'tp'), may hold values from -6 to 6
- queries: bfloat16 [65536, 1024], P(('grp', 'st'), 'tp'), parts along dimension 0, may hold values from -40 to 40
- gate_pre: bfloat16 [65536, 1024], P(('grp', 'st'), 'tp'), parts along dimension 0, may hold values from -6 to 6
- w_query: bfloat16 [2048, 1024], P(None, 'tp'), may hold values from -0.125 to 0.125
- w_gate: bfloat16 [2048, 1024], P(None, 'tp'), may hold values from -0.125 to 0.125
- w_key: bfloat16 [2048, 1024], P(None, 'tp'), may hold values from -0.125 to 0.125
- w_value: bfloat16 [2048, 1024], P(None, 'tp'), may hold values from -0.125 to 0.125
- d_mem: bfloat16 [65536, 1024], P(('grp', 'st'), 'tp'), parts along dimension 0, may hold values from -6 to 6
Outputs:
- d_tokens: bfloat16 [65536, 2048], P(('grp', 'st', 'tp')), parts along dimension 0
- d_store: bfloat16 [1024, 64, 2048], P(('grp', 'st', 'tp')), parts along dimension 0
- d_wkey: float32 [4096, 1024], P(('grp', 'st'), 'tp'), parts along dimension 0
There are 2 independent parts, one for each index of `grp`. A program takes and returns all parts, laid end to end along the dimension named above; an argument that names none is the same for every part. Nothing has to cross between parts.
Inputs may be any that keep to these rules, and one draw needn't show every extreme that they name: `pass_ids`: the 8 blocks of one index of st name at most 2 passages (counted with repetition) held by any one index of st o, that is passages o * 16 to o * 16 + 15. Every index of st takes exactly 2 passages from each of 16 indices of st and none from the others, so the bound 2 is reached by every index.
All inputs are finite; a program needn't handle non-finite values.
Results may differ from a plain program's by a relative error of at most 0.02.
Values may be sent and summed in bfloat16 or wider, within the bound.
A program may use at most 128 MiB of HBM per device.

v0:
```python
import jax
import jax.numpy as jnp
from jax import lax
from jax.sharding import Mesh
from jax.sharding import PartitionSpec as P

HD = 256
BLK = 128
PB = 4
ST = ("st_0", "st_1")
GRP_ST = ("grp", "st_0", "st_1")
GRP_ST_TP = ("grp", "st_0", "st_1", "tp")


def sum_in_order(tiles, axes, order):
    dims = [lax.axis_size(a) for a in axes]
    tiles = tiles.reshape(*dims, *tiles.shape[1:])
    tiles = tiles.transpose(*order, *range(len(axes), tiles.ndim))
    tiles = tiles.reshape(-1, *tiles.shape[len(axes) :])
    for k in order:
        tiles = lax.psum_scatter(tiles, axes[k], scatter_dimension=0, tiled=True)
    return tiles[0]


def in_blocks(array, dim, devices):
    before, after = (array.shape[:dim], array.shape[dim + 1 :])
    return jnp.moveaxis(array.reshape(*before, devices, -1, *after), dim, 0)


def summed_rows_2(array, axes, order, dim):
    devices = lax.axis_size(axes)
    return sum_in_order(in_blocks(array, dim, devices), axes, order)


def summed_on_arrival(array, axis, dim):
    devices = lax.axis_size(axis)
    tiles = lax.all_to_all(in_blocks(array, dim, devices), axis, 0, 0, tiled=True)
    return jnp.sum(tiles.astype(jnp.float32), axis=0)


def local(pass_ids, store, queries, gate_pre, w_query, w_gate, w_key, w_value, d_mem):
    st_count = lax.axis_size(ST)
    tp_count = lax.axis_size("tp")
    tok_rows, head_cols = queries.shape
    head_count = head_cols // HD
    blocks = tok_rows // BLK
    passages = store.shape[0]
    pass_len = store.shape[1]
    model_width = w_key.shape[0]
    requests = blocks * PB
    slot_depth = max(2, requests // st_count)
    slot_total = st_count * slot_depth
    pair_cols = 2 * head_cols
    request_ids = pass_ids.reshape(-1)
    owners = request_ids // passages
    within = request_ids % passages
    owner_hot = (owners[:, None] == jnp.arange(st_count, dtype=jnp.int32)[None, :]).astype(
        jnp.int32
    )
    ranking = jnp.sum(jnp.cumsum(owner_hot, axis=0) * owner_hot, axis=1) - 1
    slot_index = owners * slot_depth + ranking
    slot_hot = slot_index[:, None] == jnp.arange(slot_total, dtype=jnp.int32)[None, :]
    wanted = jnp.max(jnp.where(slot_hot, within[:, None], -1), axis=0).reshape(st_count, slot_depth)
    asked_rows = lax.all_to_all(wanted, ST, split_axis=0, concat_axis=0, tiled=True).reshape(-1)
    weight_kv = jnp.concatenate([w_key, w_value], axis=1)
    gathered = lax.all_gather(store, "tp", axis=2, tiled=True)
    flat_rows = gathered.reshape(passages * pass_len, model_width)
    kv_pass = jnp.dot(flat_rows, weight_kv, preferred_element_type=jnp.float32)
    kv_low = kv_pass.astype(jnp.bfloat16).reshape(passages, pass_len * pair_cols)
    pick_rows = (asked_rows[:, None] == jnp.arange(passages, dtype=jnp.int32)[None, :]).astype(
        jnp.bfloat16
    )
    outgoing = jnp.dot(pick_rows, kv_low, preferred_element_type=jnp.float32).astype(jnp.bfloat16)
    incoming = lax.all_to_all(
        outgoing.reshape(st_count, slot_depth, pass_len, pair_cols),
        ST,
        split_axis=0,
        concat_axis=0,
        tiled=True,
    )
    request_kv = incoming.reshape(slot_total, pass_len, pair_cols)[slot_index]
    block_kv = request_kv.reshape(blocks, PB * pass_len, pair_cols)
    key_rows = block_kv[:, :, :head_cols].reshape(blocks, PB * pass_len, head_count, HD)
    value_rows = block_kv[:, :, head_cols:].reshape(blocks, PB * pass_len, head_count, HD)
    query_rows = queries.reshape(blocks, BLK, head_count, HD)
    score_scale = HD ** (-0.5)
    scores = (
        jnp.einsum("nqhd,nkhd->nhqk", query_rows, key_rows, preferred_element_type=jnp.float32)
        * score_scale
    )
    shifted = jnp.exp(scores - jnp.max(scores, axis=-1, keepdims=True))
    prob_rows = shifted / jnp.sum(shifted, axis=-1, keepdims=True)
    probs_low = prob_rows.astype(jnp.bfloat16)
    attended = jnp.einsum(
        "nhqk,nkhd->nqhd", probs_low, value_rows, preferred_element_type=jnp.float32
    ).reshape(tok_rows, head_cols)
    gate_vals = gate_pre.astype(jnp.float32)
    sigmoid_vals = jax.nn.sigmoid(gate_vals)
    mem_grad = d_mem.astype(jnp.float32)
    attended_grad = (gate_vals * sigmoid_vals * mem_grad).astype(jnp.bfloat16)
    gate_grad = (
        mem_grad * attended * sigmoid_vals * (1.0 + gate_vals * (1.0 - sigmoid_vals))
    ).astype(jnp.bfloat16)
    attended_four = attended_grad.reshape(blocks, BLK, head_count, HD)
    prob_grad = jnp.einsum(
        "nqhd,nkhd->nhqk", attended_four, value_rows, preferred_element_type=jnp.float32
    )
    score_grad = (
        score_scale
        * prob_rows
        * (prob_grad - jnp.sum(prob_rows * prob_grad, axis=-1, keepdims=True))
    ).astype(jnp.bfloat16)
    query_grad = (
        jnp.einsum("nhqk,nkhd->nqhd", score_grad, key_rows, preferred_element_type=jnp.float32)
        .astype(jnp.bfloat16)
        .reshape(tok_rows, head_cols)
    )
    key_grad = jnp.einsum(
        "nhqk,nqhd->nkhd", score_grad, query_rows, preferred_element_type=jnp.float32
    )
    value_grad = jnp.einsum(
        "nhqk,nqhd->nkhd", probs_low, attended_four, preferred_element_type=jnp.float32
    )
    request_grads = jnp.concatenate(
        [
            key_grad.reshape(blocks, PB * pass_len, head_cols),
            value_grad.reshape(blocks, PB * pass_len, head_cols),
        ],
        axis=2,
    )
    request_grads = request_grads.astype(jnp.bfloat16).reshape(requests, pass_len * pair_cols)
    returning = jnp.dot(
        slot_hot.T.astype(jnp.bfloat16), request_grads, preferred_element_type=jnp.float32
    ).astype(jnp.bfloat16)
    arrived = lax.all_to_all(
        returning.reshape(st_count, slot_depth, pass_len, pair_cols),
        ST,
        split_axis=0,
        concat_axis=0,
        tiled=True,
    )
    pass_grad = jnp.dot(
        pick_rows.T,
        arrived.reshape(slot_total, pass_len * pair_cols),
        preferred_element_type=jnp.float32,
    )
    pass_low = pass_grad.astype(jnp.bfloat16).reshape(passages, pass_len, pair_cols)
    key_sums = pass_low[:, :, :head_cols].reshape(passages * pass_len, head_cols)
    d_wkey = summed_rows_2(
        jnp.einsum("rc,rh->ch", flat_rows, key_sums, preferred_element_type=jnp.float32),
        ST,
        (1, 0),
        0,
    )
    partial_value = pass_low.reshape(
        passages // tp_count * lax.axis_size("tp") * pass_len, pair_cols
    )
    d_store = summed_on_arrival(
        jnp.einsum("rc,dc->rd", partial_value, weight_kv, preferred_element_type=jnp.float32)
        .reshape(passages // tp_count * lax.axis_size("tp"), pass_len, model_width)
        .astype(jnp.bfloat16),
        "tp",
        0,
    ).astype(jnp.bfloat16)
    grad_both = jnp.concatenate([query_grad, gate_grad], axis=1)
    weight_both = jnp.concatenate([w_query, w_gate], axis=1)
    partial_value = grad_both
    d_tokens = summed_on_arrival(
        jnp.einsum(
            "rc,dc->rd", partial_value, weight_both, preferred_element_type=jnp.float32
        ).astype(jnp.bfloat16),
        "tp",
        0,
    ).astype(jnp.bfloat16)
    return (d_tokens, d_store, d_wkey)


def solution(mesh):
    finer = Mesh(
        mesh.devices.reshape(mesh.shape["grp"], 16, 2, mesh.shape["tp"]),
        ("grp", "st_0", "st_1", "tp"),
    )
    in_specs = (
        P(GRP_ST, None),
        P(ST, None, "tp"),
        P(GRP_ST, "tp"),
        P(GRP_ST, "tp"),
        P(None, "tp"),
        P(None, "tp"),
        P(None, "tp"),
        P(None, "tp"),
        P(GRP_ST, "tp"),
    )
    out_specs = (P(GRP_ST_TP, None), P(GRP_ST_TP, None, None), P(GRP_ST, "tp"))
    return jax.shard_map(local, mesh=finer, in_specs=in_specs, out_specs=out_specs, check_vma=False)
```

profile of v0, /device:TPU:34, one launch (start us, length us, event | category | flops | bytes accessed | tf_op | source)
XLA Modules:
  0.0 645.7 jit_solution(13220018644907863382)
XLA Ops:
  7.2 0.1 all-gather.2.cloned.1.call-start
  7.3 0.7 all-gather.2.cloned.1.call-update
  8.0 0.8 copy.65
  8.8 0.1 reshape.266
  8.9 0.1 fusion.32
  9.0 0.2 select_reduce_fusion.1
  9.2 0.1 select_reduce_fusion
  9.3 0.7 all_to_all.18
  10.0 24.7 %all-to-all-start = ((s32[32,1,2]{2,1,0:T(1,128)}), s32[32,1,2]{2,1,0:T(1,128)S(1)}, u32[]{:S(2)}, u32[]{:S(2)}) async-start(s32[32,1,2]{2,1,0:T(1,128)} %bitcast), calls=%async_computation | async-start | bytes 32768 | tf_op jit(solution)/shard_map/all_to_all | solution.py:64
  34.7 2.3 constant_dynamic-update-slice_fusion.1
  37.0 1.1 constant_dynamic-update-slice_fusion
  38.1 8.4 %all-to-all-done = s32[32,1,2]{2,1,0:T(1,128)S(1)} async-done(((s32[32,1,2]{2,1,0:T(1,128)}), s32[32,1,2]{2,1,0:T(1,128)S(1)}, u32[]{:S(2)}, u32[]{:S(2)}) %all-to-all-start) | async-done | bytes 288 | tf_op jit(solution)/shard_map/all_to_all | solution.py:64
  46.5 0.5 broadcast.215
  47.0 0.7 reduce.11
  47.7 0.1 eq.49
  47.8 29.4 %all-gather.2.cloned.1.call-done = bf16[16,64,2048]{2,1,0:T(8,128)(2,1)} async-done(((bf16[16,64,512]{2,1,0:T(8,128)(2,1)}), bf16[16,64,2048]{2,1,0:T(8,128)(2,1)}) %all-gather.2.cloned.1.call-update) | async-done | bytes 4194320 | tf_op jit(solution)/shard_map/all_gather | solution.py:66
  77.2 5.2 fusion.6
  82.4 0.5 copy.67
  83.0 0.5 reshape.268
  83.5 1.3 convolution_convert_fusion.1
  84.8 3.6 copy.87
  88.4 13.3 %all-to-all-start.1 = ((bf16[32,2,64,512]{3,2,1,0:T(8,128)(2,1)}), bf16[32,2,64,512]{3,2,1,0:T(8,128)(2,1)}, u32[]{:S(2)}, u32[]{:S(2)}) async-start(bf16[32,2,64,512]{3,2,1,0:T(8,128)(2,1)} %bitcast.76), calls=%async_computation.1 | async-start | bytes 8388608 | tf_op jit(solution)/shard_map/all_to_all | solution.py:74
  101.7 0.1 reshape.271
  101.8 183.2 %all-to-all-done.1 = bf16[32,2,64,512]{3,2,1,0:T(8,128)(2,1)} async-done(((bf16[32,2,64,512]{3,2,1,0:T(8,128)(2,1)}), bf16[32,2,64,512]{3,2,1,0:T(8,128)(2,1)}, u32[]{:S(2)}, u32[]{:S(2)}) %all-to-all-start.1) | async-done | bytes 4194336 | tf_op jit(solution)/shard_map/all_to_all | solution.py:74
  285.0 2.9 gather_fusion
  287.9 0.4 fusion.9
  288.3 1.2 copy-done.5
  289.6 1.2 fusion.36
  290.7 3.1 fusion.21
  293.8 2.9 fusion.10
  296.8 3.3 fusion.7
  300.0 1.8 multiply_reduce_fusion
  301.8 0.2 multiply_convert_fusion
  302.0 0.5 convolution_convert_fusion.6
  302.5 0.5 copy-done.9
  303.0 0.1 pad_maximum_fusion
  303.2 2.4 copy.77
  305.6 2.9 convert_element_type.78
  308.5 1.4 convolution_convert_fusion
  309.9 3.5 copy.88
  313.4 10.5 %all-to-all-start.3 = ((bf16[32,2,64,512]{3,2,1,0:T(8,128)(2,1)}), bf16[32,2,64,512]{3,2,1,0:T(8,128)(2,1)}, u32[]{:S(2)}, u32[]{:S(2)}) async-start(bf16[32,2,64,512]{3,2,1,0:T(8,128)(2,1)} %bitcast.77), calls=%async_computation.3 | async-start | bytes 8388608 | tf_op jit(solution)/shard_map/all_to_all | solution.py:135
  323.9 0.3 convolution_convert_fusion.8
  324.3 0.7 copy-done.11
  325.0 0.3 copy-done.14
  325.3 5.6 convolution_convert_fusion.4
  330.9 176.5 %all-to-all-done.3 = bf16[32,2,64,512]{3,2,1,0:T(8,128)(2,1)} async-done(((bf16[32,2,64,512]{3,2,1,0:T(8,128)(2,1)}), bf16[32,2,64,512]{3,2,1,0:T(8,128)(2,1)}, u32[]{:S(2)}, u32[]{:S(2)}) %all-to-all-start.3) | async-done | bytes 4194336 | tf_op jit(solution)/shard_map/all_to_all | solution.py:135
  507.4 6.0 all-to-all-start.2
  513.4 4.7 copy.89
  518.1 0.8 convolution_convert_fusion.2
  518.9 0.3 copy.90
  519.2 1.0 copy-done.7
  520.2 0.4 copy-done.13
  520.6 2.6 convolution_bitcast_fusion
  523.2 1.9 copy.78
  525.1 1.5 copy.79
  526.7 1.2 copy-done.8
  527.9 5.9 convolution_convert_fusion.3
  533.8 27.0 %all-to-all-done.2 = bf16[4,256,2048]{2,1,0:T(8,128)(2,1)} async-done(((bf16[4,256,2048]{2,1,0:T(8,128)(2,1)}), bf16[4,256,2048]{2,1,0:T(8,128)(2,1)}, u32[]{:S(2)}, u32[]{:S(2)}) %all-to-all-start.2) | async-done | bytes 4194336 | tf_op jit(solution)/shard_map/all_to_all | solution.py:37
  560.8 6.4 all-to-all-start.4
  567.1 0.7 reduce-scatter.5.cloned.1.call-update
  567.9 4.3 reduce_sum.54
  572.2 41.5 %all-to-all-done.4 = bf16[4,4,64,2048]{3,2,1,0:T(8,128)(2,1)} async-done(((bf16[4,4,64,2048]{3,2,1,0:T(8,128)(2,1)}), bf16[4,4,64,2048]{3,2,1,0:T(8,128)(2,1)}, u32[]{:S(2)}, u32[]{:S(2)}) %all-to-all-start.4) | async-done | bytes 4194336 | tf_op jit(solution)/shard_map/all_to_all | solution.py:37
  613.7 4.3 reduce_sum.55
  617.9 21.3 %reduce-scatter.5.cloned.1.call-done = f32[1,64,256]{2,1,0:T(8,128)} async-done(((f32[16,64,256]{2,1,0:T(8,128)}), f32[1,64,256]{2,1,0:T(8,128)}) %reduce-scatter.5.cloned.1.call-update) | async-done | bytes 65552 | tf_op jit(solution)/shard_map/reduce_scatter | solution.py:21
  (32 shorter events, 0.2 us)
Async XLA Ops:
  7.2 280.7 %copy-start = (bf16[1024,256]{1,0:T(8,128)(2,1)S(1)}, bf16[1024,256]{1,0:T(8,128)(2,1)}, u32[]{:S(2)}) copy-start(bf16[1024,256]{1,0:T(8,128)(2,1)} %param.11) | copy-start | bytes 1572868
  7.2 29.8 %copy-start.6 = (bf16[2048,256]{1,0:T(8,128)(2,1)S(1)}, bf16[2048,256]{1,0:T(8,128)(2,1)}, u32[]{:S(2)}) copy-start(bf16[2048,256]{1,0:T(8,128)(2,1)} %param.16) | copy-start | bytes 3145732
  7.2 70.0 %all-gather.2.cloned.1.call-start = ((), (), s32[]{:S(2)}) async-start(), calls=%async_computation.7 | async-start | bytes 5242880 | tf_op jit(solution)/shard_map/all_gather | solution.py:66
  10.0 36.5 %all-to-all-start = ((s32[32,1,2]{2,1,0:T(1,128)}), s32[32,1,2]{2,1,0:T(1,128)S(1)}, u32[]{:S(2)}, u32[]{:S(2)}) async-start(s32[32,1,2]{2,1,0:T(1,128)} %bitcast), calls=%async_computation | async-start | bytes 32768 | tf_op jit(solution)/shard_map/all_to_all | solution.py:64
  88.4 196.6 %all-to-all-start.1 = ((bf16[32,2,64,512]{3,2,1,0:T(8,128)(2,1)}), bf16[32,2,64,512]{3,2,1,0:T(8,128)(2,1)}, u32[]{:S(2)}, u32[]{:S(2)}) async-start(bf16[32,2,64,512]{3,2,1,0:T(8,128)(2,1)} %bitcast.76), calls=%async_computation.1 | async-start | bytes 8388608 | tf_op jit(solution)/shard_map/all_to_all | solution.py:74
  287.9 12.1 %copy-start.2 = (bf16[32,64,512]{2,1,0:T(8,128)(2,1)}, bf16[32,64,512]{2,1,0:T(8,128)(2,1)S(1)}, u32[]{:S(2)}) copy-start(bf16[32,64,512]{2,1,0:T(8,128)(2,1)S(1)} %gather_fusion) | copy-start | bytes 6291460
  288.3 1.2 copy-start.5
  290.7 3.1 copy-start.10
  296.8 3.3 copy-start.12
  300.0 1.8 copy-start.4
  301.8 1.2 copy-start.9
  313.4 10.5 %copy-start.3 = (bf16[32,64,512]{2,1,0:T(8,128)(2,1)S(1)}, bf16[32,64,512]{2,1,0:T(8,128)(2,1)}, u32[]{:S(2)}) copy-start(bf16[32,64,512]{2,1,0:T(8,128)(2,1)} %copy-done.2) | copy-start | bytes 6291460
  313.4 194.0 %all-to-all-start.3 = ((bf16[32,2,64,512]{3,2,1,0:T(8,128)(2,1)}), bf16[32,2,64,512]{3,2,1,0:T(8,128)(2,1)}, u32[]{:S(2)}, u32[]{:S(2)}) async-start(bf16[32,2,64,512]{3,2,1,0:T(8,128)(2,1)} %bitcast.77), calls=%async_computation.3 | async-start | bytes 8388608 | tf_op jit(solution)/shard_map/all_to_all | solution.py:135
  323.9 1.0 copy-start.11
  323.9 1.4 copy-start.14
  507.4 53.4 %all-to-all-start.2 = ((bf16[4,256,2048]{2,1,0:T(8,128)(2,1)}), bf16[4,256,2048]{2,1,0:T(8,128)(2,1)}, u32[]{:S(2)}, u32[]{:S(2)}) async-start(bf16[4,256,2048]{2,1,0:T(8,128)(2,1)} %bitcast.87), calls=%async_computation.2 | async-start | bytes 8388608 | tf_op jit(solution)/shard_map/all_to_all | solution.py:37
  513.4 53.7 %reduce-scatter.3.cloned.1.call-start = ((), (), s32[]{:S(2)}) async-start(), calls=%async_computation.8 | async-start | bytes 3145728 | tf_op jit(solution)/shard_map/reduce_scatter | solution.py:21
  518.1 2.5 copy-start.13
  519.2 1.0 copy-start.7
  526.7 1.2 copy-start.8
  560.8 52.9 %all-to-all-start.4 = ((bf16[4,4,64,2048]{3,2,1,0:T(8,128)(2,1)}), bf16[4,4,64,2048]{3,2,1,0:T(8,128)(2,1)}, u32[]{:S(2)}, u32[]{:S(2)}) async-start(bf16[4,4,64,2048]{3,2,1,0:T(8,128)(2,1)} %bitcast.88), calls=%async_computation.4 | async-start | bytes 8388608 | tf_op jit(solution)/shard_map/all_to_all | solution.py:37
  567.1 72.1 %reduce-scatter.5.cloned.1.call-start = ((), (), s32[]{:S(2)}) async-start(), calls=%async_computation.9 | async-start | bytes 1114112 | tf_op jit(solution)/shard_map/reduce_scatter | solution.py:21
  567.9 71.3 %copy-start.1 = (bf16[1024,256]{1,0:T(8,128)(2,1)S(1)}, bf16[1024,256]{1,0:T(8,128)(2,1)}, u32[]{:S(2)}) copy-start(bf16[1024,256]{1,0:T(8,128)(2,1)} %param.11) | copy-start | bytes 1572868
Sparse Core Ops, SparseCore 0:
  9.9 67.3 all-gather.1
  526.9 17.2 reduce-scatter.2
  571.0 68.1 reduce-scatter.4
where the time goes:
time: 647 us; the launch traced here: 646 us
  waiting for transfers between devices  489 us (76%)
  starting transfers between devices  61 us (9%)
  local copies, waits for them, and re-layouts  35.7 us (6%)
  matrix products  32.1 us (5%)
  other arithmetic  14.1 us (2%)
  between operations  14.1 us (2%)
    all_to_all x1, waiting for transfers between devices, local(): lax.all_to_all(outgoing.reshape(st_count, slot_depth, pass_len, pair_cols...  183 us
    all_to_all x1, waiting for transfers between devices, local(): lax.all_to_all(returning.reshape(st_count, slot_depth, pass_len, pair_col...  176 us
    all_to_all x2, waiting for transfers between devices, summed_on_arrival(): lax.all_to_all(in_blocks(array, dim, devices), axis, 0, 0, tiled=True)  68.5 us
    all_gather x1, waiting for transfers between devices, local(): gathered = lax.all_gather(store, 'tp', axis=2, tiled=True)  29.4 us
    all_to_all x1, starting transfers between devices, local(): lax.all_to_all(wanted, ST, split_axis=0, concat_axis=0, tiled=True)  24.7 us
    reduce_scatter x2, waiting for transfers between devices, sum_in_order(): tiles = lax.psum_scatter(tiles, axes[k], scatter_dimension=0, tiled=True)  21.3 us
    unnamed x36, local copies, waits for them, and re-layouts  20.5 us
    all_to_all x1, starting transfers between devices, local(): lax.all_to_all(outgoing.reshape(st_count, slot_depth, pass_len, pair_cols...  13.3 us
  transfers between devices with their start and end apart: 8, of which 7 were waited for; matrix products, arithmetic and copies ran while one was open for 6% of the time, Pallas kernels for 0%

commit v1 on v0

--- a/solution.py
+++ b/solution.py
@@ -39,6 +39,18 @@
 
 
 def local(pass_ids, store, queries, gate_pre, w_query, w_gate, w_key, w_value, d_mem):
+
+    def attach_the_row(panel, lane_axis):
+        return jnp.concatenate(
+            lax.all_to_all(
+                jnp.stack([panel for _ in range(lax.axis_size(lane_axis))], 0),
+                axis_name=lane_axis,
+                split_axis=0,
+                concat_axis=0,
+            ),
+            2,
+        )
+
     st_count = lax.axis_size(ST)
     tp_count = lax.axis_size("tp")
     tok_rows, head_cols = queries.shape
@@ -63,7 +75,7 @@
     wanted = jnp.max(jnp.where(slot_hot, within[:, None], -1), axis=0).reshape(st_count, slot_depth)
     asked_rows = lax.all_to_all(wanted, ST, split_axis=0, concat_axis=0, tiled=True).reshape(-1)
     weight_kv = jnp.concatenate([w_key, w_value], axis=1)
-    gathered = lax.all_gather(store, "tp", axis=2, tiled=True)
+    gathered = attach_the_row(store, lane_axis="tp")
     flat_rows = gathered.reshape(passages * pass_len, model_width)
     kv_pass = jnp.dot(flat_rows, weight_kv, preferred_element_type=jnp.float32)
     kv_low = kv_pass.astype(jnp.bfloat16).reshape(passages, pass_len * pair_cols)

time: 647 us -> 675 us (1.043)
  blocking collectives: 0 us -> 36.4 us
  starting transfers between devices: 61 us -> 29.4 us
  waiting for transfers between devices: 489 us -> 502 us
  local copies, waits for them, and re-layouts: 35.7 us -> 47.3 us
    all_to_all x0 -> x1, blocking collectives: none -> 36.4 us  [local(): lax.all_to_all(wanted, ST, split_axis=0, concat_axis=0, tiled=True)]
    all_to_all x1, waiting for transfers between devices: 8.36 us -> 43.7 us  [attach_the_row(): lax.all_to_all(jnp.stack([panel for _ in range(lax.axis_size(lane_axis))]...]
    all_gather x1 -> x0, waiting for transfers between devices: 29.4 us -> none  [local(): gathered = lax.all_gather(store, 'tp', axis=2, tiled=True)]
    all_to_all x1, starting transfers between devices: 24.7 us -> 5.36 us  [attach_the_row(): lax.all_to_all(jnp.stack([panel for _ in range(lax.axis_size(lane_axis))]...]
    all_to_all x2, waiting for transfers between devices: 68.5 us -> 56 us  [summed_on_arrival(): lax.all_to_all(in_blocks(array, dim, devices), axis, 0, 0, tiled=True)]
    all_to_all x1, starting transfers between devices: 13.3 us -> 5.84 us  [local(): lax.all_to_all(outgoing.reshape(st_count, slot_depth, pass_len, pair_cols...]
    all_to_all x1, waiting for transfers between devices: 176 us -> 184 us  [local(): lax.all_to_all(returning.reshape(st_count, slot_depth, pass_len, pair_col...]
    all_to_all x1, waiting for transfers between devices: 183 us -> 190 us  [local(): lax.all_to_all(outgoing.reshape(st_count, slot_depth, pass_len, pair_cols...]
  transfers between devices with their start and end apart: 8 -> 7, of which waited for: 7 -> 6; matrix products, arithmetic and copies ran while one was open for 6% -> 5% of each run, Pallas kernels for 0% -> 0%
where the time goes in v1:
time: 675 us; the launch traced here: 674 us
  waiting for transfers between devices  502 us (74%)
  local copies, waits for them, and re-layouts  47.3 us (7%)
  blocking collectives  36.4 us (5%)
  matrix products  30.9 us (5%)
  starting transfers between devices  29.4 us (4%)
  between operations  14.4 us (2%)
  other arithmetic  14.1 us (2%)
    all_to_all x1, waiting for transfers between devices, local(): lax.all_to_all(outgoing.reshape(st_count, slot_depth, pass_len, pair_cols...  190 us
    all_to_all x1, waiting for transfers between devices, local(): lax.all_to_all(returning.reshape(st_count, slot_depth, pass_len, pair_col...  184 us
    all_to_all x2, waiting for transfers between devices, summed_on_arrival(): lax.all_to_all(in_blocks(array, dim, devices), axis, 0, 0, tiled=True)  56 us
    all_to_all x1, waiting for transfers between devices, attach_the_row(): lax.all_to_all(jnp.stack([panel for _ in range(lax.axis_size(lane_axis))]...  43.7 us
    all_to_all x1, blocking collectives, local(): lax.all_to_all(wanted, ST, split_axis=0, concat_axis=0, tiled=True)  36.4 us
    reduce_scatter x2, waiting for transfers between devices, sum_in_order(): tiles = lax.psum_scatter(tiles, axes[k], scatter_dimension=0, tiled=True)  27.2 us
    unnamed x41, local copies, waits for them, and re-layouts  23.1 us
  transfers between devices with their start and end apart: 7, of which 6 were waited for; matrix products, arithmetic and copies ran while one was open for 5% of the time, Pallas kernels for 0%

profile of v1, /device:TPU:34, one launch (start us, length us, event | category | flops | bytes accessed | tf_op | source)
XLA Modules:
  0.0 674.2 jit_solution(18394513524802144891)
XLA Ops:
  7.2 0.8 copy.66
  8.2 0.2 select_reduce_fusion.1
  8.4 0.1 select_reduce_fusion
  8.5 0.1 all_to_all.21
  8.6 36.4 %all_to_all.34 = s32[32,1,2]{2,1,0:T(1,128)S(1)} all-to-all(s32[32,1,2]{2,1,0:T(1,128)S(1)} %bitcast.102), channel_id=1, replica_groups=mesh['grp'=2,'st_0'=16,'st_1'=2,'tp'=4] {'st_0','st_1'}, dimensions={0} | all-to-all | bytes 512 | tf_op jit(solution)/shard_map/all_to_all | solution.py:76
  45.0 3.8 stack.2
  48.7 5.4 all-to-all-start.1
  54.1 1.1 constant_dynamic-update-slice_fusion.1
  55.2 0.5 copy-done.11
  55.7 1.1 constant_dynamic-update-slice_fusion
  56.8 0.5 broadcast.217
  57.3 0.7 reduce.11
  58.0 0.1 eq.49
  58.1 43.7 %all-to-all-done.1 = bf16[4,16,64,512]{3,2,1,0:T(8,128)(2,1)} async-done(((bf16[4,16,64,512]{3,2,1,0:T(8,128)(2,1)}), bf16[4,16,64,512]{3,2,1,0:T(8,128)(2,1)}, u32[]{:S(2)}, u32[]{:S(2)}) %all-to-all-start.1) | async-done | bytes 4194336 | tf_op jit(solution)/shard_map/all_to_all | solution.py:45
  101.8 5.7 copy.68
  107.5 1.4 copy.89
  109.0 1.9 copy-done.4
  110.9 4.0 fusion.6
  114.8 0.5 copy.69
  115.4 0.5 reshape.272
  115.9 1.3 convolution_convert_fusion.1
  117.2 3.6 copy.90
  120.8 5.8 all-to-all-start.2
  126.7 190.3 %all-to-all-done.2 = bf16[32,2,64,512]{3,2,1,0:T(8,128)(2,1)} async-done(((bf16[32,2,64,512]{3,2,1,0:T(8,128)(2,1)}), bf16[32,2,64,512]{3,2,1,0:T(8,128)(2,1)}, u32[]{:S(2)}, u32[]{:S(2)}) %all-to-all-start.2) | async-done | bytes 4194336 | tf_op jit(solution)/shard_map/all_to_all | solution.py:86
  317.1 2.9 gather_fusion
  320.0 0.4 fusion.9
  320.4 1.2 copy-done.7
  321.6 1.2 fusion.35
  322.8 3.1 fusion.21
  325.9 2.9 fusion.10
  328.8 3.3 fusion.7
  332.1 1.8 multiply_reduce_fusion
  333.9 0.2 multiply_convert_fusion
  334.1 0.5 convolution_convert_fusion.6
  334.6 0.5 copy-done.12
  335.1 0.1 pad_maximum_fusion
  335.3 2.4 copy.79
  337.7 2.9 convert_element_type.78
  340.6 1.4 convolution_convert_fusion
  341.9 3.5 copy.91
  345.5 5.8 all-to-all-start.4
  351.3 0.3 convolution_convert_fusion.8
  351.7 0.7 copy-done.14
  352.3 0.3 copy-done.16
  352.7 5.6 convolution_convert_fusion.4
  358.3 183.7 %all-to-all-done.4 = bf16[32,2,64,512]{3,2,1,0:T(8,128)(2,1)} async-done(((bf16[32,2,64,512]{3,2,1,0:T(8,128)(2,1)}), bf16[32,2,64,512]{3,2,1,0:T(8,128)(2,1)}, u32[]{:S(2)}, u32[]{:S(2)}) %all-to-all-start.4) | async-done | bytes 4194336 | tf_op jit(solution)/shard_map/all_to_all | solution.py:147
  541.9 6.1 all-to-all-start.3
  548.0 4.7 copy.92
  552.7 0.8 convolution_convert_fusion.2
  553.5 0.3 copy.93
  553.9 1.0 copy-done.8
  554.9 0.3 copy-done.5
  555.2 2.6 convolution_bitcast_fusion
  557.8 1.9 copy.80
  559.8 1.5 copy.81
  561.4 1.2 copy-done.9
  562.5 5.9 convolution_convert_fusion.3
  568.4 20.8 %all-to-all-done.3 = bf16[4,256,2048]{2,1,0:T(8,128)(2,1)} async-done(((bf16[4,256,2048]{2,1,0:T(8,128)(2,1)}), bf16[4,256,2048]{2,1,0:T(8,128)(2,1)}, u32[]{:S(2)}, u32[]{:S(2)}) %all-to-all-start.3) | async-done | bytes 4194336 | tf_op jit(solution)/shard_map/all_to_all | solution.py:37
  589.2 6.4 all-to-all-start.5
  595.5 0.8 reduce-scatter.5.cloned.1.call-update
  596.3 4.3 reduce_sum.54
  600.6 35.2 %all-to-all-done.5 = bf16[4,4,64,2048]{3,2,1,0:T(8,128)(2,1)} async-done(((bf16[4,4,64,2048]{3,2,1,0:T(8,128)(2,1)}), bf16[4,4,64,2048]{3,2,1,0:T(8,128)(2,1)}, u32[]{:S(2)}, u32[]{:S(2)}) %all-to-all-start.5) | async-done | bytes 4194336 | tf_op jit(solution)/shard_map/all_to_all | solution.py:37
  635.8 4.3 reduce_sum.55
  640.1 27.2 %reduce-scatter.5.cloned.1.call-done = f32[1,64,256]{2,1,0:T(8,128)} async-done(((f32[16,64,256]{2,1,0:T(8,128)}), f32[1,64,256]{2,1,0:T(8,128)}) %reduce-scatter.5.cloned.1.call-update) | async-done | bytes 65552 | tf_op jit(solution)/shard_map/reduce_scatter | solution.py:21
  (38 shorter events, 0.5 us)
Async XLA Ops:
  7.2 312.8 %copy-start = (bf16[1024,256]{1,0:T(8,128)(2,1)S(1)}, bf16[1024,256]{1,0:T(8,128)(2,1)}, u32[]{:S(2)}) copy-start(bf16[1024,256]{1,0:T(8,128)(2,1)} %param.11) | copy-start | bytes 1572868
  48.7 5.4 copy-start.10
  48.7 53.1 %all-to-all-start.1 = ((bf16[4,16,64,512]{3,2,1,0:T(8,128)(2,1)}), bf16[4,16,64,512]{3,2,1,0:T(8,128)(2,1)}, u32[]{:S(2)}, u32[]{:S(2)}) async-start(bf16[4,16,64,512]{3,2,1,0:T(8,128)(2,1)} %stack.2), calls=%async_computation.1 | async-start | bytes 8388608 | tf_op jit(solution)/shard_map/all_to_all | solution.py:45
  54.1 1.6 copy-start.11
  108.9 1.9 copy-start.4
  120.8 196.3 %all-to-all-start.2 = ((bf16[32,2,64,512]{3,2,1,0:T(8,128)(2,1)}), bf16[32,2,64,512]{3,2,1,0:T(8,128)(2,1)}, u32[]{:S(2)}, u32[]{:S(2)}) async-start(bf16[32,2,64,512]{3,2,1,0:T(8,128)(2,1)} %bitcast.79), calls=%async_computation.2 | async-start | bytes 8388608 | tf_op jit(solution)/shard_map/all_to_all | solution.py:86
  320.0 12.2 %copy-start.2 = (bf16[32,64,512]{2,1,0:T(8,128)(2,1)}, bf16[32,64,512]{2,1,0:T(8,128)(2,1)S(1)}, u32[]{:S(2)}) copy-start(bf16[32,64,512]{2,1,0:T(8,128)(2,1)S(1)} %gather_fusion) | copy-start | bytes 6291460
  320.4 1.2 copy-start.7
  322.8 3.1 copy-start.13
  328.8 3.3 copy-start.15
  332.1 1.8 copy-start.6
  333.9 1.2 copy-start.12
  345.5 5.8 copy-start.3
  345.5 196.4 %all-to-all-start.4 = ((bf16[32,2,64,512]{3,2,1,0:T(8,128)(2,1)}), bf16[32,2,64,512]{3,2,1,0:T(8,128)(2,1)}, u32[]{:S(2)}, u32[]{:S(2)}) async-start(bf16[32,2,64,512]{3,2,1,0:T(8,128)(2,1)} %bitcast.80), calls=%async_computation.4 | async-start | bytes 8388608 | tf_op jit(solution)/shard_map/all_to_all | solution.py:147
  351.3 1.0 copy-start.14
  351.3 1.4 copy-start.16
  541.9 47.3 %all-to-all-start.3 = ((bf16[4,256,2048]{2,1,0:T(8,128)(2,1)}), bf16[4,256,2048]{2,1,0:T(8,128)(2,1)}, u32[]{:S(2)}, u32[]{:S(2)}) async-start(bf16[4,256,2048]{2,1,0:T(8,128)(2,1)} %bitcast.93), calls=%async_computation.3 | async-start | bytes 8388608 | tf_op jit(solution)/shard_map/all_to_all | solution.py:37
  548.0 47.5 %reduce-scatter.3.cloned.1.call-start = ((), (), s32[]{:S(2)}) async-start(), calls=%async_computation.8 | async-start | bytes 3145728 | tf_op jit(solution)/shard_map/reduce_scatter | solution.py:21
  552.7 2.5 copy-start.5
  553.9 1.0 copy-start.8
  561.3 1.2 copy-start.9
  589.2 46.7 %all-to-all-start.5 = ((bf16[4,4,64,2048]{3,2,1,0:T(8,128)(2,1)}), bf16[4,4,64,2048]{3,2,1,0:T(8,128)(2,1)}, u32[]{:S(2)}, u32[]{:S(2)}) async-start(bf16[4,4,64,2048]{3,2,1,0:T(8,128)(2,1)} %bitcast.94), calls=%async_computation.5 | async-start | bytes 8388608 | tf_op jit(solution)/shard_map/all_to_all | solution.py:37
  595.5 71.8 %reduce-scatter.5.cloned.1.call-start = ((), (), s32[]{:S(2)}) async-start(), calls=%async_computation.9 | async-start | bytes 1114112 | tf_op jit(solution)/shard_map/reduce_scatter | solution.py:21
  596.3 71.0 %copy-start.1 = (bf16[1024,256]{1,0:T(8,128)(2,1)S(1)}, bf16[1024,256]{1,0:T(8,128)(2,1)}, u32[]{:S(2)}) copy-start(bf16[1024,256]{1,0:T(8,128)(2,1)} %param.11) | copy-start | bytes 1572868
Sparse Core Ops, SparseCore 0:
  561.5 10.7 reduce-scatter.2
  599.4 67.8 reduce-scatter.4
